TPU v7x, 32 devices: a whole 2x2x4 slice. The times are simulated.
32 devices in a mesh: ep: 8 (over z, core), tp: 4 (over y, x).
Axes of the slice: x: 2, y: 2, z: 4, core: 2. Of those that a mesh axis runs over, the one named last changes fastest.
Arguments:
- tokens: bfloat16 [128, 2048], P('ep'), may hold values from -6 to 6
- old_state: bfloat16 [128, 256, 2048], P('ep', None, 'tp'), may hold values from -3 to 3
- first_gain: bfloat16 [2048], replicated, may hold values from 0.099609375 to 1.8984375
- query_weight: bfloat16 [2048, 1024], P('tp'), may hold values from -0.125 to 0.125
- key_weight: bfloat16 [2048, 1024], P('tp'), may hold values from -0.125 to 0.125
- value_weight: bfloat16 [2048, 2048], P(None, 'tp'), may hold values from -0.125 to 0.125
- outgate_weight: bfloat16 [2048, 2048], P(None, 'tp'), may hold values from -0.125 to 0.125
- lowrank_weight: bfloat16 [2048, 16], replicated, may hold values from -0.125 to 0.125
- decay_weight: bfloat16 [16, 1024], replicated, may hold values from -20 to 20
- decay_bias: float32 [1024], replicated, may hold values from -40 to 2
- head_gain: bfloat16 [2048], P('tp'), may hold values from 0.099609375 to 1.8984375
- output_weight: bfloat16 [2048, 2048], P('tp'), may hold values from -0.125 to 0.125
- second_gain: bfloat16 [2048], replicated, may hold values from 0.099609375 to 1.8984375
- expert_gate: bfloat16 [8, 2048, 1920], P('ep', None, 'tp'), may hold values from -0.125 to 0.125
- expert_up: bfloat16 [8, 2048, 1920], P('ep', None, 'tp'), may hold values from -0.125 to 0.125
- expert_down: bfloat16 [8, 1920, 2048], P('ep', 'tp'), may hold values from -0.125 to 0.125
- shared_gate: bfloat16 [2048, 1920], P(None, 'tp'), may hold values from -0.125 to 0.125
- shared_up: bfloat16 [2048, 1920], P(None, 'tp'), may hold values from -0.125 to 0.125
- shared_down: bfloat16 [1920, 2048], P('tp'), may hold values from -0.125 to 0.125
- route_ids: int32 [128, 4], P('ep'), may hold values from 0 to 7, all different within a row; in each aligned block of 16 rows (0 to 15, 16 to 31, ...) at most 16 rows name the same one
- route_weights: float32 [128, 4], P('ep'), may hold values from 0.1 to 1
Outputs:
- layer_out: bfloat16 [128, 2048], P('ep', 'tp')
- new_state: bfloat16 [128, 256, 2048], P('ep', None, 'tp')
Inputs may be any that keep to these rules, and one draw needn't show every extreme that they name: `route_ids`: within the rows of one device (aligned blocks of 16 rows) no expert is named more than 16 times, a bound that some block reaches.
All inputs are finite; a program needn't handle non-finite values.
Results may differ from a plain program's by a relative error of at most 0.035.
Values may be sent and summed in bfloat16 or wider, within the bound.
A program may use at most 64 MiB of HBM per device.

v0:
```python
import jax
import jax.numpy as jnp
from jax import lax
from jax.sharding import PartitionSpec as P

EPSILON = 1e-06


def rms_norm(values, norm_gain):
    floats = values.astype(jnp.float32)
    scaled = floats * lax.rsqrt(jnp.mean(floats * floats, axis=-1, keepdims=True) + EPSILON)
    return (scaled * norm_gain.astype(jnp.float32)).astype(jnp.bfloat16)


def project(left_side, right_side):
    return jnp.dot(left_side, right_side, preferred_element_type=jnp.float32)


def body(
    tokens,
    old_state,
    first_gain,
    query_weight,
    key_weight,
    value_weight,
    outgate_weight,
    lowrank_weight,
    decay_weight,
    decay_bias,
    head_gain,
    output_weight,
    second_gain,
    expert_gate,
    expert_up,
    expert_down,
    shared_gate,
    shared_up,
    shared_down,
    route_ids,
    route_weights,
):
    tp_count = lax.axis_size("tp")
    ep_count = lax.axis_size("ep")
    tp_index = lax.axis_index("tp")
    seq_count, model_width = tokens.shape
    key_width = old_state.shape[1]
    value_count = old_state.shape[2]
    head_count = decay_weight.shape[1] // key_width
    head_width = value_count * tp_count // head_count
    head_index = tp_index * value_count // head_width
    feature_cols = model_width // tp_count
    normed = rms_norm(tokens, first_gain)
    own_normed = lax.dynamic_slice_in_dim(normed, tp_index * feature_cols, feature_cols, 1)
    query_sum, key_sum = (
        lax.psum(project(own_normed, query_weight).astype(jnp.bfloat16), "tp").astype(jnp.float32),
        lax.psum(project(own_normed, key_weight).astype(jnp.bfloat16), "tp").astype(jnp.float32),
    )
    offset = head_index * key_width
    query_rows = lax.dynamic_slice_in_dim(query_sum.astype(jnp.bfloat16), offset, key_width, 1)
    key_rows = lax.dynamic_slice_in_dim(key_sum.astype(jnp.bfloat16), offset, key_width, 1)
    value_rows = project(normed, value_weight).astype(jnp.bfloat16)
    out_gate = project(normed, outgate_weight).astype(jnp.bfloat16)
    lowrank = project(normed, lowrank_weight).astype(jnp.bfloat16)
    decay_cols = lax.dynamic_slice_in_dim(decay_weight, offset, key_width, 1)
    bias_cols = lax.dynamic_slice_in_dim(decay_bias, offset, key_width, 0)
    log_decay = jax.nn.log_sigmoid(project(lowrank, decay_cols) + bias_cols) / 16.0
    carried = (
        jnp.exp(log_decay)[:, :, None] * old_state.astype(jnp.float32)
        + key_rows.astype(jnp.float32)[:, :, None] * value_rows.astype(jnp.float32)[:, None, :]
    )
    new_state = carried.astype(jnp.bfloat16)
    read_out = jnp.einsum(
        "bi,bic->bc", query_rows.astype(jnp.float32), carried, precision=lax.Precision.HIGHEST
    ) * key_width ** (-0.5)
    own_squares = jnp.sum(read_out * read_out, axis=1)
    mixed_rows = (
        read_out * head_gain.astype(jnp.float32) * jax.nn.silu(out_gate.astype(jnp.float32))
    ).astype(jnp.bfloat16)
    partial_value = project(mixed_rows, output_weight)
    selector = (jnp.arange(head_count) == head_index).astype(jnp.float32)
    head_squares = own_squares[:, None] * selector[None, :]
    head_sums, square_sums = (
        lax.psum(
            (partial_value[:, None, :] * selector[None, :, None]).astype(jnp.bfloat16), "tp"
        ).astype(jnp.float32),
        lax.psum(head_squares.astype(jnp.bfloat16), "tp").astype(jnp.float32),
    )
    inverse = lax.rsqrt(square_sums / head_width + EPSILON)
    attended = jnp.sum(head_sums * inverse[:, :, None], axis=1)
    second = (tokens.astype(jnp.float32) + attended).astype(jnp.bfloat16)
    normed_two = rms_norm(second, second_gain)
    shared_hidden = (
        jax.nn.silu(project(normed_two, shared_gate)) * project(normed_two, shared_up)
    ).astype(jnp.bfloat16)
    shared_own = lax.psum_scatter(
        project(shared_hidden, shared_down).astype(jnp.bfloat16),
        "tp",
        scatter_dimension=1,
        tiled=True,
    ).astype(jnp.float32)
    local_experts = expert_gate.shape[0]
    expert_count = local_experts * ep_count
    top_count = route_ids.shape[1]
    capacity = max(2, (2 * seq_count * top_count + expert_count - 1) // expert_count)
    flat_ids = route_ids.reshape(-1)
    onehot = (flat_ids[:, None] == jnp.arange(expert_count, dtype=jnp.int32)[None, :]).astype(
        jnp.int32
    )
    slot_rank = jnp.sum((jnp.cumsum(onehot, axis=0) - onehot) * onehot, axis=1)
    target = flat_ids * capacity + slot_rank
    placing = (
        target[None, :] == jnp.arange(expert_count * capacity, dtype=jnp.int32)[:, None]
    ).astype(jnp.bfloat16)
    dispatched = project(placing, jnp.repeat(normed_two, top_count, axis=0)).astype(jnp.bfloat16)
    dispatched = dispatched.reshape(expert_count, capacity, normed_two.shape[1])
    received = lax.all_to_all(dispatched, "ep", split_axis=0, concat_axis=0, tiled=True)
    slot_count = received.shape[1]
    grouped = received.reshape(ep_count, local_experts, slot_count, model_width)
    grouped = grouped.transpose(1, 0, 2, 3).reshape(
        local_experts, ep_count * slot_count, model_width
    )
    gate_vals = jnp.einsum("erd,edf->erf", grouped, expert_gate, preferred_element_type=jnp.float32)
    up_vals = jnp.einsum("erd,edf->erf", grouped, expert_up, preferred_element_type=jnp.float32)
    hidden = (jax.nn.silu(gate_vals) * up_vals).astype(jnp.bfloat16)
    down_vals = jnp.einsum("erf,efd->erd", hidden, expert_down, preferred_element_type=jnp.float32)
    summed = lax.psum_scatter(down_vals.astype(jnp.bfloat16), "tp", scatter_dimension=2, tiled=True)
    regrouped = summed.reshape(local_experts, ep_count, slot_count, feature_cols)
    regrouped = regrouped.transpose(1, 0, 2, 3).reshape(expert_count, slot_count, feature_cols)
    returned = lax.all_to_all(regrouped, "ep", split_axis=0, concat_axis=0, tiled=True)
    picked = returned.reshape(expert_count * capacity, feature_cols)[target]
    picked = picked.astype(jnp.float32).reshape(seq_count, top_count, feature_cols)
    routed = jnp.sum(picked * route_weights[:, :, None], axis=1)
    own_second = lax.dynamic_slice_in_dim(second, tp_index * feature_cols, feature_cols, 1).astype(
        jnp.float32
    )
    layer_out = (own_second + shared_own + routed).astype(jnp.bfloat16)
    return (layer_out, new_state)


def solution(mesh):
    placed = (
        P("ep", None),
        P("ep", None, "tp"),
        P(),
        P("tp", None),
        P("tp", None),
        P(None, "tp"),
        P(None, "tp"),
        P(),
        P(),
        P(),
        P("tp"),
        P("tp", None),
        P(),
        P("ep", None, "tp"),
        P("ep", None, "tp"),
        P("ep", "tp", None),
        P(None, "tp"),
        P(None, "tp"),
        P("tp", None),
        P("ep", None),
        P("ep", None),
    )
    return jax.shard_map(
        body,
        mesh=mesh,
        in_specs=placed,
        out_specs=(P("ep", "tp"), P("ep", None, "tp")),
        check_vma=False,
    )
```

profile of v0, /device:TPU:0, one launch (start us, length us, event | category | flops | bytes accessed | tf_op | source)
XLA Modules:
  0.0 198.8 jit_solution(12057159878163100648)
XLA Ops:
  7.2 0.0 copy-start
  7.2 0.0 copy-start.5
  7.2 0.0 copy-start.3
  7.2 0.0 copy-start.2
  7.2 0.0 all-reduce.6.cloned.1.call-start
  7.3 1.1 fusion.31
  8.4 0.7 convert_element_type.126
  9.1 0.9 fusion.33
  10.0 0.0 copy-start.6
  10.0 2.1 %convolution_convert_fusion.3 = bf16[16,1024]{1,0:T(8,128)(2,1)} fusion(bf16[512,1024]{1,0:T(8,128)(2,1)} %param.25, bf16[16,2048]{1,0:T(8,128)(2,1)S(1)} %fusion.33, s32[]{:T(128)S(6)} %select_n.30), kind=kOutput, calls=%fused_computation.18 | convolution fusion | flops 16793600 | bytes 1097732 | tf_op jit(solution)/shard_map/dot_general | solution.py:16
  12.1 2.1 %convolution_convert_fusion.4 = bf16[16,1024]{1,0:T(8,128)(2,1)} fusion(bf16[512,1024]{1,0:T(8,128)(2,1)} %param.24, bf16[16,2048]{1,0:T(8,128)(2,1)S(1)} %fusion.33, s32[]{:T(128)S(6)} %select_n.30), kind=kOutput, calls=%fused_computation.19 | convolution fusion | flops 16793600 | bytes 1097732 | tf_op jit(solution)/shard_map/dot_general | solution.py:16
  14.2 0.0 all-reduce.6.cloned.1.call-update
  14.2 0.0 all-reduce.4.cloned.1.call-start
  14.3 0.0 copy-done.5
  14.4 0.1 copy.29
  14.4 0.1 reshape.122
  14.5 0.1 fusion.41
  14.6 0.1 reduce_window_sum.11
  14.7 0.2 select_reduce_fusion
  14.9 2.0 fusion.19
  16.9 0.8 dynamic_slice.21
  17.6 1.0 fusion.51
  18.7 40.3 %all-reduce.6.cloned.1.call-done = (bf16[16,1024]{1,0:T(8,128)(2,1)}, bf16[16,1024]{1,0:T(8,128)(2,1)}) async-done(((bf16[16,1024]{1,0:T(8,128)(2,1)}, bf16[16,1024]{1,0:T(8,128)(2,1)}), (bf16[16,1024]{1,0:T(8,128)(2,1)}, bf16[16,1024]{1,0:T(8,128)(2,1)})) %all-reduce.6.cloned.1.call-update) | async-done | bytes 65552 | tf_op jit(solution)/shard_map/psum | solution.py:56
  59.0 0.7 dynamic-slice_convert_fusion
  59.7 0.7 dynamic-slice_bitcast_fusion
  60.4 5.6 %fusion.1 = f32[16,1,512]{2,1,0:T(1,128)S(1)} fusion(bf16[16,256,512]{2,1,0:T(8,128)(2,1)} %param.22, f32[16,512]{1,0:T(8,128)S(1)} %fusion.19, f32[16,256]{1,0:T(8,128)S(1)} %dynamic-slice_convert_fusion, f32[16,256]{1,0:T(8,128)S(1)} %fusion.51, bf16[16,256,1]{1,0,2:T(8,128)(2,1)S(1)} %dynamic-slice_bitcast_fusion), kind=kOutput, calls=%fused_computation.3 | convolution fusion | flops 33554432 | bytes 4300800 | tf_op jit(solution)/shard_map/bi,bic->bc/dot_general | solution.py:72
  66.0 0.1 fusion.39
  66.2 0.0 copy-done
  66.2 0.0 copy-start.1
  66.2 2.4 %fusion.47 = f32[16,2048]{1,0:T(8,128)S(1)} fusion(bf16[512,2048]{1,0:T(8,128)(2,1)S(1)} %copy-done, bf16[16,2048]{1,0:T(8,128)(2,1)S(1)} %fusion.33, bf16[2048,512]{1,0:T(8,128)(2,1)} %param.27, f32[16,1,512]{2,1,0:T(1,128)S(1)} %fusion.1, f32[512]{0:T(512)S(1)} %convert_multiply_fusion.4), kind=kOutput, calls=%fused_computation.68 | convolution fusion | flops 67182592 | bytes 4425728 | tf_op jit(solution)/shard_map/dot_general | solution.py:16
  68.6 0.8 multiply_convert_fusion
  69.4 0.0 all-reduce.4.cloned.1.call-update
  69.4 0.0 reduce-scatter.5.cloned.1.call-start
  69.4 0.1 multiply_convert_fusion.1
  69.5 8.9 %psum.31 = bf16[16,4]{0,1:T(4,128)(2,1)S(1)} all-reduce(bf16[16,4]{0,1:T(4,128)(2,1)S(1)} %multiply_convert_fusion.1), channel_id=1, replica_groups=mesh['ep'=8,'tp'=4] {'tp'}, use_global_device_ids=true, to_apply=%region_5.6 | all-reduce | flops 64 | bytes 256 | tf_op jit(solution)/shard_map/psum | solution.py:86
  78.4 34.2 %all-reduce.4.cloned.1.call-done = bf16[16,4,2048]{2,0,1:T(8,128)(2,1)} async-done(((bf16[16,4,2048]{2,0,1:T(8,128)(2,1)}), bf16[16,4,2048]{2,0,1:T(8,128)(2,1)}) %all-reduce.4.cloned.1.call-update) | async-done | bytes 262160 | tf_op jit(solution)/shard_map/psum | solution.py:83
  112.6 1.1 multiply_reduce_fusion
  113.7 0.0 copy-done.1
  113.7 0.1 fusion.28
  113.9 0.1 fusion.30
  114.0 0.1 broadcast_in_dim.2
  114.1 0.1 reshape.123
  114.1 0.3 convolution_convert_fusion.1
  114.4 19.7 %all_to_all.10 = bf16[8,16,2048]{2,1,0:T(8,128)(2,1)S(1)} all-to-all(bf16[8,16,2048]{2,1,0:T(8,128)(2,1)S(1)} %bitcast.62), channel_id=1, replica_groups=mesh['ep'=8,'tp'=4] {'ep'}, dimensions={0} | all-to-all | bytes 1048576 | tf_op jit(solution)/shard_map/all_to_all | solution.py:116
  134.2 2.2 %fusion.9 = f32[128,480]{0,1:T(8,128)S(1)} fusion(bf16[128,2048]{1,0:T(8,128)(2,1)S(1)} %bitcast.59, bf16[1,2048,480]{1,2,0:T(8,128)(2,1)} %param.34), kind=kOutput, calls=%fused_computation.14 | convolution fusion | flops 251658240 | bytes 2736128 | tf_op jit(solution)/shard_map/erd,edf->erf/dot_general | solution.py:122
  136.4 0.0 copy-start.4
  136.4 4.6 %fusion.5 = bf16[1,128,2048]{2,1,0:T(8,128)(2,1)} fusion(bf16[1,480,2048]{2,1,0:T(8,128)(2,1)} %param.36, bf16[128,2048]{1,0:T(8,128)(2,1)S(1)} %bitcast.60, bf16[1,2048,480]{1,2,0:T(8,128)(2,1)} %param.35, f32[128,480]{0,1:T(8,128)S(1)} %fusion.9), kind=kOutput, calls=%fused_computation.9 | convolution fusion | flops 503947264 | bytes 5226496 | tf_op jit(solution)/shard_map/erf,efd->erd/dot_general | solution.py:125
  141.0 0.0 reduce-scatter.5.cloned.1.call-update
  141.0 0.0 reduce-scatter.3.cloned.1.call-start
  141.1 0.1 copy.30
  141.1 0.1 mul.223
  141.2 0.0 copy-done.4
  141.2 0.1 copy.31
  141.3 2.2 %fusion.67 = f32[16,480]{1,0:T(8,128)S(1)} fusion(bf16[16,2048]{1,0:T(8,128)(2,1)S(1)} %fusion.30, bf16[2048,480]{0,1:T(8,128)(2,1)} %param.37), kind=kOutput, calls=%fused_computation.100 | convolution fusion | flops 31457280 | bytes 2062336 | tf_op jit(solution)/shard_map/dot_general | solution.py:16
  143.5 3.8 %convolution_convert_fusion.2 = bf16[16,2048]{1,0:T(8,128)(2,1)} fusion(bf16[480,2048]{1,0:T(8,128)(2,1)} %param.39, bf16[16,2048]{1,0:T(8,128)(2,1)S(1)} %fusion.30, bf16[2048,480]{0,1:T(8,128)(2,1)} %param.38, f32[16,480]{1,0:T(8,128)S(1)} %fusion.67), kind=kOutput, calls=%fused_computation.10 | convolution fusion | flops 62993408 | bytes 4093952 | tf_op jit(solution)/shard_map/dot_general | solution.py:16
  147.3 0.0 reduce-scatter.3.cloned.1.call-update
  147.4 16.8 %reduce-scatter.5.cloned.1.call-done = bf16[1,128,512]{2,1,0:T(8,128)(2,1)} async-done(((bf16[1,128,2048]{2,1,0:T(8,128)(2,1)}), bf16[1,128,512]{2,1,0:T(8,128)(2,1)}) %reduce-scatter.5.cloned.1.call-update) | async-done | bytes 131088 | tf_op jit(solution)/shard_map/reduce_scatter | solution.py:126
  164.2 4.6 %all-to-all-start.1 = ((bf16[8,16,512]{2,1,0:T(8,128)(2,1)}), bf16[8,16,512]{2,1,0:T(8,128)(2,1)S(1)}, u32[]{:S(2)}, u32[]{:S(2)}) async-start(bf16[8,16,512]{2,1,0:T(8,128)(2,1)} %bitcast.63), calls=%async_computation.3 | async-start | bytes 262144 | tf_op jit(solution)/shard_map/all_to_all | solution.py:129
  168.8 4.4 %fusion = bf16[16,256,512]{2,1,0:T(8,128)(2,1)} fusion(bf16[16,256,512]{2,1,0:T(8,128)(2,1)} %param.22, f32[16,512]{1,0:T(8,128)S(1)} %fusion.19, f32[16,256]{1,0:T(8,128)S(1)} %dynamic-slice_convert_fusion, f32[16,256]{1,0:T(8,128)S(1)} %fusion.51), kind=kLoop, calls=%fused_computation.2 | loop fusion | flops 10485760 | bytes 8454144 | tf_op jit(solution)/shard_map/convert_element_type | solution.py:71
  173.2 2.3 %all-to-all-done.1 = bf16[8,16,512]{2,1,0:T(8,128)(2,1)S(1)} async-done(((bf16[8,16,512]{2,1,0:T(8,128)(2,1)}), bf16[8,16,512]{2,1,0:T(8,128)(2,1)S(1)}, u32[]{:S(2)}, u32[]{:S(2)}) %all-to-all-start.1) | async-done | bytes 131104 | tf_op jit(solution)/shard_map/all_to_all | solution.py:129
  175.6 0.7 gather_fusion
  176.3 0.1 multiply_reduce_fusion.1
  176.5 14.4 %reduce-scatter.3.cloned.1.call-done = bf16[16,512]{1,0:T(8,128)(2,1)} async-done(((bf16[16,2048]{1,0:T(8,128)(2,1)}), bf16[16,512]{1,0:T(8,128)(2,1)}) %reduce-scatter.3.cloned.1.call-update) | async-done | bytes 16400 | tf_op jit(solution)/shard_map/reduce_scatter | solution.py:95
  190.9 1.3 add_convert_fusion
  (14 shorter events, 0.1 us)
Async XLA Ops:
  7.2 59.0 %copy-start = (bf16[512,2048]{1,0:T(8,128)(2,1)S(1)}, bf16[512,2048]{1,0:T(8,128)(2,1)}, u32[]{:S(2)}) copy-start(bf16[512,2048]{1,0:T(8,128)(2,1)} %param.32) | copy-start | bytes 6291460
  7.2 7.1 %copy-start.5 = (bf16[512]{0:T(512)(128)(2,1)S(1)}, bf16[512]{0:T(512)(128)(2,1)}, u32[]{:S(2)}) copy-start(bf16[512]{0:T(512)(128)(2,1)} %param.31) | copy-start | bytes 3076
  7.2 7.1 %copy-start.3 = (bf16[2048]{0:T(1024)(128)(2,1)S(1)}, bf16[2048]{0:T(1024)(128)(2,1)}, u32[]{:S(2)}) copy-start(bf16[2048]{0:T(1024)(128)(2,1)} %param.33) | copy-start | bytes 12292
  7.2 7.1 %copy-start.2 = (s32[16,4]{0,1:T(4,128)S(1)}, s32[16,4]{0,1:T(4,128)}, u32[]{:S(2)}) copy-start(s32[16,4]{0,1:T(4,128)} %param.40) | copy-start | bytes 772
  7.2 51.8 %all-reduce.6.cloned.1.call-start = ((), (), s32[]{:S(2)}) async-start(), calls=%async_computation.7 | async-start | bytes 131072 | tf_op jit(solution)/shard_map/psum | solution.py:56
  10.0 7.7 %copy-start.6 = (bf16[2048,16]{0,1:T(8,128)(2,1)S(1)}, bf16[2048,16]{0,1:T(8,128)(2,1)}, u32[]{:S(2)}) copy-start(bf16[2048,16]{0,1:T(8,128)(2,1)} %param.28) | copy-start | bytes 196612
  14.2 98.4 %all-reduce.4.cloned.1.call-start = ((), (), s32[]{:S(2)}) async-start(), calls=%async_computation.4 | async-start | bytes 524288 | tf_op jit(solution)/shard_map/psum | solution.py:83
  66.2 47.5 %copy-start.1 = (bf16[16,2048]{1,0:T(8,128)(2,1)S(1)}, bf16[16,2048]{1,0:T(8,128)(2,1)}, u32[]{:S(2)}) copy-start(bf16[16,2048]{1,0:T(8,128)(2,1)} %param.21) | copy-start | bytes 196612
  69.4 94.8 %reduce-scatter.5.cloned.1.call-start = ((), (), s32[]{:S(2)}) async-start(), calls=%async_computation.6 | async-start | bytes 655360 | tf_op jit(solution)/shard_map/reduce_scatter | solution.py:126
  136.4 4.8 %copy-start.4 = (f32[16,4]{0,1:T(4,128)S(1)}, f32[16,4]{0,1:T(4,128)}, u32[]{:S(2)}) copy-start(f32[16,4]{0,1:T(4,128)} %param.41) | copy-start | bytes 772
  141.0 49.9 %reduce-scatter.3.cloned.1.call-start = ((), (), s32[]{:S(2)}) async-start(), calls=%async_computation.5 | async-start | bytes 81920 | tf_op jit(solution)/shard_map/reduce_scatter | solution.py:95
  164.2 11.4 %all-to-all-start.1 = ((bf16[8,16,512]{2,1,0:T(8,128)(2,1)}), bf16[8,16,512]{2,1,0:T(8,128)(2,1)S(1)}, u32[]{:S(2)}, u32[]{:S(2)}) async-start(bf16[8,16,512]{2,1,0:T(8,128)(2,1)} %bitcast.63), calls=%async_computation.3 | async-start | bytes 262144 | tf_op jit(solution)/shard_map/all_to_all | solution.py:129
Sparse Core Ops, SparseCore 0:
  14.4 44.5 all-reduce.5
  69.5 43.0 all-reduce.3
  141.1 23.0 reduce-scatter.4
  166.8 24.0 reduce-scatter.2
where the time goes:
time: 200 us; the launch traced here: 199 us
  waiting for transfers between devices  108 us (54%)
  blocking collectives  28.6 us (14%)
  matrix products  28.2 us (14%)
  between operations  14 us (7%)
  other arithmetic  12 us (6%)
  starting transfers between devices  4.77 us (2%)
  local copies, waits for them, and re-layouts  2.85 us (1%)
    psum x1, waiting for transfers between devices, body(): lax.psum(project(own_normed, key_weight).astype(jnp.bfloat16), 'tp')  40.3 us
    psum x1, waiting for transfers between devices, body(): lax.psum((partial_value[:, None, :] * selector[None, :, None]).astype(jnp...  34.2 us
    all_to_all x1, blocking collectives, body(): lax.all_to_all(dispatched, 'ep', split_axis=0, concat_axis=0, tiled=True)  19.7 us
    reduce_scatter x1, waiting for transfers between devices, body(): lax.psum_scatter(down_vals.astype(jnp.bfloat16), 'tp', scatter_dimension=...  16.8 us
    dot_general x8, matrix products, project(): return jnp.dot(left_side, right_side, preferred_element_type=jnp.float32)  15.8 us
    reduce_scatter x1, waiting for transfers between devices, body(): lax.psum_scatter(project(shared_hidden, shared_down).astype(jnp.bfloat16)...  14.4 us
    psum x1, blocking collectives, body(): lax.psum(head_squares.astype(jnp.bfloat16), 'tp').astype(jnp.float32)  8.91 us
    dot_general x1, matrix products, body(): jnp.einsum('bi,bic->bc', query_rows.astype(jnp.float32), carried, precisi...  5.64 us
  transfers between devices with their start and end apart: 5, of which 5 were waited for; matrix products, arithmetic and copies ran while one was open for 8% of the time, Pallas kernels for 0%

commit v1 on v0

v1 whole, which is shorter than its diff:
```python
import functools

import jax
import jax.numpy as jnp
from jax import lax
from jax.experimental import pallas as pl
from jax.experimental.pallas import tpu as pltpu
from jax.sharding import PartitionSpec as P

EPSILON = 1e-06
MESH = pl.DeviceIdType.MESH
F32 = jnp.float32
BF16 = jnp.bfloat16


def silu(v):
    return v / (1.0 + jnp.exp(-v))


def norm_rows(floats, gain):
    scale = lax.rsqrt(jnp.mean(floats * floats, axis=-1, keepdims=True) + EPSILON)
    return (floats * scale * gain.astype(F32)).astype(BF16)


def dot(left, right):
    return jnp.dot(left, right, preferred_element_type=F32)


def layer_kernel(
    n_ep, n_tp, heads,
    tokens, first_gain, lowrank_w, decay_w, decay_b, head_gain, second_gain, ids, weights,
    state_h, qw_h, kw_h, vw_h, gw_h, ow_h, eg_h, eu_h, ed_h, sg_h, su_h, sd_h,
    out, new_state_h,
    qw, kw, vw, gw, ow, eg, eu, ed, sg, su, sd, state, load_sem, store_sem,
    normed, qk_part, qk_send, qk_recv, values, row_cols,
    at_send, at_recv, sq_send, sq_recv, second, rows_in, down_send, down_recv,
    sh_send, sh_recv, back_send, back_recv,
    qk_s, qk_r, at_s, at_r, sq_s, sq_r, z_s, z_r, c_s, c_r, dn_s, dn_r, sh_s, sh_r, bk_s, bk_r,
):
    ep = lax.axis_index("ep")
    tp = lax.axis_index("tp")
    zs = n_ep // 2
    z, core = ep // 2, ep % 2
    batch, width = tokens.shape
    key_width, value_count = state.shape[1], state.shape[2]
    feats = width // n_tp
    head_width = value_count * n_tp // heads
    rows = n_ep * batch

    def tp_peer(d):
        return lax.rem(tp + d, n_tp)

    def ep_at(dz, r):
        return lax.rem(z - dz + zs, zs) * 2 + (core if r == 0 else 1 - core)

    def remote(src, dst, ssem, rsem, ep_to, tp_to):
        return pltpu.make_async_remote_copy(
            src_ref=src, dst_ref=dst, send_sem=ssem, recv_sem=rsem,
            device_id=(ep_to, tp_to), device_id_type=MESH,
        )

    barrier = pltpu.get_barrier_semaphore()
    for d in range(1, n_tp):
        pl.semaphore_signal(barrier, inc=1, device_id=(ep, tp_peer(d)), device_id_type=MESH)
    for d in range(1, n_ep):
        pl.semaphore_signal(
            barrier, inc=1, device_id=(lax.rem(ep + d, n_ep), tp), device_id_type=MESH
        )

    sources = [
        (qw_h, qw), (kw_h, kw), (vw_h, vw), (gw_h, gw), (state_h, state), (ow_h, ow),
        (sg_h, sg), (su_h, su), (sd_h, sd), (eg_h.at[0], eg), (eu_h.at[0], eu), (ed_h.at[0], ed),
    ]
    loads = {}
    for i, (src, dst) in enumerate(sources):
        copy = pltpu.make_async_copy(src, dst, load_sem.at[i])
        copy.start()
        loads[id(dst)] = copy

    def arrived(ref):
        loads[id(ref)].wait()

    tok = tokens[...].astype(F32)
    nrm = norm_rows(tok, first_gain[...])
    normed[...] = nrm
    own = normed[:, pl.ds(pl.multiple_of(tp * feats, 128), feats)]
    qk_cols = heads * key_width
    arrived(qw)
    qk_part[:, :qk_cols] = dot(own, qw[...]).astype(BF16)
    arrived(kw)
    qk_part[:, qk_cols:] = dot(own, kw[...]).astype(BF16)

    def qk_block(peer):
        off = pl.multiple_of((peer * value_count // head_width) * key_width, 128)
        return (
            qk_part[:, pl.ds(off, key_width)],
            qk_part[:, pl.ds(pl.multiple_of(qk_cols + off, 128), key_width)],
        )

    pl.semaphore_wait(barrier, n_tp - 1 + n_ep - 1)

    qk_copies = []
    for d in range(1, n_tp):
        peer = tp_peer(d)
        qb, kb = qk_block(peer)
        qk_send[d, :, :key_width] = qb
        qk_send[d, :, key_width:] = kb
        cp = remote(qk_send.at[d], qk_recv.at[d], qk_s.at[d], qk_r.at[d], ep, peer)
        cp.start()
        qk_copies.append(cp)

    offset = pl.multiple_of((tp * value_count // head_width) * key_width, 128)
    lowrank = dot(nrm, lowrank_w[...]).astype(BF16)
    pre = dot(lowrank, decay_w[:, pl.ds(offset, key_width)]) + decay_b[:, pl.ds(offset, key_width)]
    log_decay = (jnp.minimum(pre, 0.0) - jnp.log1p(jnp.exp(-jnp.abs(pre)))) / 16.0
    decay = jnp.exp(log_decay)
    arrived(vw)
    val = dot(nrm, vw[...]).astype(BF16).astype(F32)
    values[...] = val
    arrived(gw)
    gate = dot(nrm, gw[...]).astype(BF16).astype(F32)
    gated = head_gain[...].astype(F32) * silu(gate)

    q_own, k_own = qk_block(tp)
    query = q_own.astype(F32)
    key = k_own.astype(F32)
    for d in range(1, n_tp):
        qk_copies[d - 1].wait_recv()
        query = query + qk_recv[d, :, :key_width].astype(F32)
        key = key + qk_recv[d, :, key_width:].astype(F32)
    query = query.astype(BF16).astype(F32)
    key = key.astype(BF16).astype(F32)

    scaled = query * decay
    high = scaled.astype(BF16)
    low = (scaled - high.astype(F32)).astype(BF16)
    left = jnp.concatenate([high, low], axis=0)
    row_id = lax.broadcasted_iota(jnp.int32, (batch, value_count), 0)
    arrived(state)

    def read_one(b, acc):
        both = dot(left, state[b])
        return jnp.where(row_id == b, both[:batch] + both[batch:], acc)

    acc = lax.fori_loop(0, batch, read_one, jnp.zeros((batch, value_count), F32), unroll=4)
    qk = jnp.sum(query * key, axis=1, keepdims=True)
    read_out = (acc + qk * val) * key_width ** (-0.5)
    squares = jnp.sum(read_out * read_out, axis=1, keepdims=True)
    mixed = (read_out * gated).astype(BF16)

    if value_count != head_width:
        sq_send[...] = jnp.broadcast_to(squares, sq_send.shape)
        sq_copies = []
        for d in range(1, n_tp):
            cp = remote(sq_send, sq_recv.at[d], sq_s.at[d], sq_r.at[d], ep, tp_peer(d))
            cp.start()
            sq_copies.append(cp)
        my_head = tp * value_count // head_width
        for d in range(1, n_tp):
            sq_copies[d - 1].wait_recv()
            src_head = lax.rem(tp - d + n_tp, n_tp) * value_count // head_width
            same = jnp.where(src_head == my_head, 1.0, 0.0).astype(F32)
            squares = squares + same * sq_recv[d][:, :1]
        for cp in sq_copies:
            cp.wait_send()
    inverse = lax.rsqrt(squares / head_width + EPSILON)

    arrived(ow)
    partial = (dot(mixed, ow[...]) * inverse).astype(BF16)
    at_send[...] = partial
    at_copies = []
    for d in range(1, n_tp):
        cp = remote(at_send, at_recv.at[d], at_s.at[d], at_r.at[d], ep, tp_peer(d))
        cp.start()
        at_copies.append(cp)

    stacked = jnp.concatenate([key, decay, jnp.zeros((128 - 2 * batch, key_width), F32)], axis=0)
    row_cols[...] = stacked.T
    lane = lax.broadcasted_iota(jnp.int32, (key_width, 128), 1)
    step = 32

    def update(b, carry):
        cols = row_cols[...]
        key_col = jnp.sum(jnp.where(lane == b, cols, 0.0), axis=1, keepdims=True)
        dec_col = jnp.sum(jnp.where(lane == b + batch, cols, 0.0), axis=1, keepdims=True)
        value_row = values[pl.ds(b, 1), :]
        for i in range(0, key_width, step):
            old = state[b, i : i + step, :].astype(F32)
            new = dec_col[i : i + step] * old + key_col[i : i + step] * value_row
            state[b, i : i + step, :] = new.astype(BF16)
        return carry

    half = batch // 2
    lax.fori_loop(0, half, update, 0)

    total = tok + 0.0
    attended = partial.astype(F32)
    for d in range(1, n_tp):
        at_copies[d - 1].wait_recv()
        attended = attended + at_recv[d].astype(F32)
    sec = (total + attended).astype(BF16)
    second[...] = sec
    nrm2 = norm_rows(sec.astype(F32), second_gain[...])
    rows_in[0] = nrm2

    z_copies = []
    for dz in range(1, zs):
        cp = remote(
            rows_in.at[0], rows_in.at[2 * dz], z_s.at[dz], z_r.at[dz],
            lax.rem(z + dz, zs) * 2 + core, tp,
        )
        cp.start()
        z_copies.append(cp)
    sibling = z * 2 + 1 - core
    c_copies = [remote(rows_in.at[0], rows_in.at[1], c_s.at[0], c_r.at[0], sibling, tp)]
    c_copies[0].start()

    arrived(sg)
    arrived(su)
    hid = (silu(dot(nrm2, sg[...])) * dot(nrm2, su[...])).astype(BF16)
    arrived(sd)
    sh_copies = []
    for d in list(range(1, n_tp)) + [0]:
        peer = tp_peer(d)
        part = dot(hid, sd[:, pl.ds(pl.multiple_of(peer * feats, 128), feats)]).astype(BF16)
        sh_send[d] = part
        if d > 0:
            cp = remote(sh_send.at[d], sh_recv.at[d], sh_s.at[d], sh_r.at[d], ep, peer)
            cp.start()
            sh_copies.append(cp)

    lax.fori_loop(half, batch, update, 0)
    store = pltpu.make_async_copy(state, new_state_h, store_sem)
    store.start()

    for dz in range(1, zs):
        z_copies[dz - 1].wait_recv()
        cp = remote(
            rows_in.at[2 * dz], rows_in.at[2 * dz + 1], c_s.at[dz], c_r.at[dz], sibling, tp
        )
        cp.start()
        c_copies.append(cp)
    arrived(eg)
    arrived(eu)
    arrived(ed)
    for cp in c_copies:
        cp.wait_recv()

    x = rows_in[...].reshape(rows, width)
    hidden = (silu(dot(x, eg[...])) * dot(x, eu[...])).astype(BF16)
    down_copies = []
    for d in list(range(1, n_tp)) + [0]:
        peer = tp_peer(d)
        part = dot(hidden, ed[:, pl.ds(pl.multiple_of(peer * feats, 128), feats)]).astype(BF16)
        down_send[d] = part
        if d > 0:
            cp = remote(down_send.at[d], down_recv.at[d], dn_s.at[d], dn_r.at[d], ep, peer)
            cp.start()
            down_copies.append(cp)
    summed = down_send[0].astype(F32)
    for d in range(1, n_tp):
        down_copies[d - 1].wait_recv()
        summed = summed + down_recv[d].astype(F32)
    back_send[...] = summed.astype(BF16).reshape(n_ep, batch, feats)

    back_copies = []
    for slot in range(1, n_ep):
        dz, r = slot // 2, slot % 2
        cp = remote(
            back_send.at[slot], back_recv.at[slot], bk_s.at[slot], bk_r.at[slot], ep_at(dz, r), tp
        )
        cp.start()
        back_copies.append(cp)

    shared = sh_send[0].astype(F32)
    for d in range(1, n_tp):
        sh_copies[d - 1].wait_recv()
        shared = shared + sh_recv[d].astype(F32)
    result = shared + second[:, pl.ds(pl.multiple_of(tp * feats, 128), feats)].astype(F32)
    id_vals = ids[...]
    w_vals = weights[...]
    for slot in range(n_ep):
        dz, r = slot // 2, slot % 2
        if slot == 0:
            piece = back_send[0]
        else:
            back_copies[slot - 1].wait_recv()
            piece = back_recv[slot]
        expert = lax.rem(z + dz, zs) * 2 + (core if r == 0 else 1 - core)
        share = jnp.sum(jnp.where(id_vals == expert, w_vals, 0.0), axis=1, keepdims=True)
        result = result + share * piece.astype(F32)
    out[...] = result.astype(BF16)

    for cp in qk_copies + at_copies + z_copies + c_copies + sh_copies + down_copies + back_copies:
        cp.wait_send()
    store.wait()


def body(
    n_ep, n_tp,
    tokens, old_state, first_gain, query_weight, key_weight, value_weight, outgate_weight,
    lowrank_weight, decay_weight, decay_bias, head_gain, output_weight, second_gain,
    expert_gate, expert_up, expert_down, shared_gate, shared_up, shared_down,
    route_ids, route_weights,
):
    batch, width = tokens.shape
    key_width, value_count = old_state.shape[1], old_state.shape[2]
    heads = decay_weight.shape[1] // key_width
    feats = width // n_tp
    qk_cols = heads * key_width
    rows = n_ep * batch
    zs = n_ep // 2
    vmem = pl.BlockSpec(memory_space=pltpu.VMEM)
    hbm = pl.BlockSpec(memory_space=pl.ANY)
    dma = pltpu.SemaphoreType.DMA
    big = [
        query_weight, key_weight, value_weight, outgate_weight, output_weight,
        expert_gate[0], expert_up[0], expert_down[0], shared_gate, shared_up, shared_down,
    ]
    scratch = [pltpu.VMEM(w.shape, BF16) for w in big]
    scratch += [
        pltpu.VMEM(old_state.shape, BF16),
        dma((12,)),
        dma,
        pltpu.VMEM((batch, width), BF16),
        pltpu.VMEM((batch, 2 * qk_cols), BF16),
        pltpu.VMEM((n_tp, batch, 2 * key_width), BF16),
        pltpu.VMEM((n_tp, batch, 2 * key_width), BF16),
        pltpu.VMEM((batch, value_count), F32),
        pltpu.VMEM((key_width, 128), F32),
        pltpu.VMEM((batch, width), BF16),
        pltpu.VMEM((n_tp, batch, width), BF16),
        pltpu.VMEM((batch, 128), F32),
        pltpu.VMEM((n_tp, batch, 128), F32),
        pltpu.VMEM((batch, width), BF16),
        pltpu.VMEM((n_ep, batch, width), BF16),
        pltpu.VMEM((n_tp, rows, feats), BF16),
        pltpu.VMEM((n_tp, rows, feats), BF16),
        pltpu.VMEM((n_tp, batch, feats), BF16),
        pltpu.VMEM((n_tp, batch, feats), BF16),
        pltpu.VMEM((n_ep, batch, feats), BF16),
        pltpu.VMEM((n_ep, batch, feats), BF16),
    ]
    for count in (n_tp, n_tp, n_tp, zs, zs, n_tp, n_tp, n_ep):
        scratch += [dma((count,)), dma((count,))]
    layer_out, new_state = pl.pallas_call(
        functools.partial(layer_kernel, n_ep, n_tp, heads),
        out_shape=(
            jax.ShapeDtypeStruct((batch, feats), BF16),
            jax.ShapeDtypeStruct(old_state.shape, BF16),
        ),
        in_specs=[vmem] * 9 + [hbm] * 12,
        out_specs=(vmem, hbm),
        scratch_shapes=scratch,
        compiler_params=pltpu.CompilerParams(
            collective_id=0, has_side_effects=True, vmem_limit_bytes=60 * 1024 * 1024
        ),
    )(
        tokens, first_gain[None], lowrank_weight, decay_weight, decay_bias[None],
        head_gain[None], second_gain[None], route_ids, route_weights,
        old_state, query_weight, key_weight, value_weight, outgate_weight, output_weight,
        expert_gate, expert_up, expert_down, shared_gate, shared_up, shared_down,
    )
    return layer_out, new_state


def solution(mesh):
    placed = (
        P("ep", None),
        P("ep", None, "tp"),
        P(),
        P("tp", None),
        P("tp", None),
        P(None, "tp"),
        P(None, "tp"),
        P(),
        P(),
        P(),
        P("tp"),
        P("tp", None),
        P(),
        P("ep", None, "tp"),
        P("ep", None, "tp"),
        P("ep", "tp", None),
        P(None, "tp"),
        P(None, "tp"),
        P("tp", None),
        P("ep", None),
        P("ep", None),
    )
    return jax.shard_map(
        functools.partial(body, mesh.shape["ep"], mesh.shape["tp"]),
        mesh=mesh,
        in_specs=placed,
        out_specs=(P("ep", "tp"), P("ep", None, "tp")),
        check_vma=False,
    )
```

time: 200 us -> 66.8 us (0.33)
  waiting for transfers between devices: 108 us -> 0 us
  Pallas kernels: 0 us -> 38.5 us
  blocking collectives: 28.6 us -> 0 us
  matrix products: 28.2 us -> 0 us
  local copies, waits for them, and re-layouts: 2.85 us -> 27.2 us
  between operations: 14 us -> 0.65 us
  other arithmetic: 12 us -> 0 us
  starting transfers between devices: 4.77 us -> 0 us
    psum x2 -> x0, waiting for transfers between devices: 74.5 us -> none  [the longest x1 40.3 us: body(): lax.psum(project(own_normed, key_weight).astype(jnp.bfloat16), 'tp')]
    pallas_call x0 -> x1, Pallas kernels: none -> 38.5 us  [body(): pl.pallas_call(functools.partial(layer_kernel, n_ep, n_tp, heads), out_sh...]
    reduce_scatter x2 -> x0, waiting for transfers between devices: 31.3 us -> none  [the longest x1 16.8 us: body(): lax.psum_scatter(down_vals.astype(jnp.bfloat16), 'tp', scatter_dimension=...]
    dot_general x11 -> x0, matrix products: 28.2 us -> none  [the longest x8 15.8 us: project(): return jnp.dot(left_side, right_side, preferred_element_type=jnp.float32)]
    unnamed x16 -> x13, local copies, waits for them, and re-layouts: 0.21 us -> 23.4 us
    all_to_all x1 -> x0, blocking collectives: 19.7 us -> none  [body(): lax.all_to_all(dispatched, 'ep', split_axis=0, concat_axis=0, tiled=True)]
    convert_element_type x11 -> x0, other arithmetic: 9.11 us -> none  [the longest x1 4.42 us: body(): new_state = carried.astype(jnp.bfloat16)]
    psum x1 -> x0, blocking collectives: 8.91 us -> none  [body(): lax.psum(head_squares.astype(jnp.bfloat16), 'tp').astype(jnp.float32)]
  transfers between devices with their start and end apart: 5 -> 0, of which waited for: 5 -> 0; matrix products, arithmetic and copies ran while one was open for 8% -> 0% of each run, Pallas kernels for 0% -> 0%
where the time goes in v1:
time: 66.8 us; the launch traced here: 66.3 us
  Pallas kernels  38.5 us (58%)
  local copies, waits for them, and re-layouts  27.2 us (41%)
    pallas_call x1, Pallas kernels, body(): pl.pallas_call(functools.partial(layer_kernel, n_ep, n_tp, heads), out_sh...  38.5 us
    unnamed x13, local copies, waits for them, and re-layouts  23.4 us

profile of v1, /device:TPU:0, one launch (start us, length us, event | category | flops | bytes accessed | tf_op | source)
XLA Modules:
  0.0 66.3 jit_solution(10161774990921947342)
XLA Ops:
  0.6 1.3 %broadcast_in_dim.14.head_gain = bf16[1,512]{1,0:T(2,128)(2,1)} reshape(bf16[512]{0:T(512)(128)(2,1)} %param.31) | data formatting | bytes 2048 | tf_op jit(solution)/shard_map/broadcast_in_dim | solution.py:360
  1.9 1.3 %broadcast_in_dim.12.first_gain = bf16[1,2048]{1,0:T(2,128)(2,1)} reshape(bf16[2048]{0:T(1024)(128)(2,1)} %param.23) | data formatting | bytes 8192 | tf_op jit(solution)/shard_map/broadcast_in_dim | solution.py:359
  3.2 1.3 %broadcast_in_dim.15.second_gain = bf16[1,2048]{1,0:T(2,128)(2,1)} reshape(bf16[2048]{0:T(1024)(128)(2,1)} %param.33) | data formatting | bytes 8192 | tf_op jit(solution)/shard_map/broadcast_in_dim | solution.py:360
  4.5 1.4 %copy.24.ids = s32[16,4]{1,0:T(8,128)} copy(s32[16,4]{0,1:T(4,128)} %param.40) | data formatting | bytes 512 | tf_op args[19]
  5.8 1.3 %copy.25.weights = f32[16,4]{1,0:T(8,128)} copy(f32[16,4]{0,1:T(4,128)} %param.41) | data formatting | bytes 512 | tf_op args[20]
  7.2 1.9 %copy.23.lowrank_w = bf16[2048,16]{1,0:T(8,128)(2,1)} copy(bf16[2048,16]{0,1:T(8,128)(2,1)} %param.28) | data formatting | bytes 131072 | tf_op args[7]
  9.0 0.0 copy-start
  9.0 4.0 %copy.26.eg_h = bf16[1,2048,480]{2,1,0:T(8,128)(2,1)} copy(bf16[1,2048,480]{1,2,0:T(8,128)(2,1)} %param.34) | data formatting | bytes 3932160 | tf_op args[13]
  13.0 0.0 copy-done
  13.0 2.4 %copy.27.eu_h = bf16[1,2048,480]{2,1,0:T(8,128)(2,1)} copy(bf16[1,2048,480]{1,2,0:T(8,128)(2,1)S(1)} %copy-done) | data formatting | bytes 3932160 | tf_op args[14]
  15.5 0.0 copy-start.1
  15.5 4.0 %copy.28.sg_h = bf16[2048,480]{1,0:T(8,128)(2,1)} copy(bf16[2048,480]{0,1:T(8,128)(2,1)} %param.37) | data formatting | bytes 3932160 | tf_op args[16]
  19.5 0.0 copy-done.1
  19.5 2.4 %copy.29.su_h = bf16[2048,480]{1,0:T(8,128)(2,1)} copy(bf16[2048,480]{0,1:T(8,128)(2,1)S(1)} %copy-done.1) | data formatting | bytes 3932160 | tf_op args[17]
  22.0 38.5 %shard_map.212 = (bf16[16,512]{1,0:T(8,128)(2,1)}, bf16[16,256,512]{2,1,0:T(8,128)(2,1)}) custom-call(bf16[16,2048]{1,0:T(8,128)(2,1)} %tokens.1, bf16[1,2048]{1,0:T(2,128)(2,1)} %broadcast_in_dim.12.first_gain, bf16[2048,16]{1,0:T(8,128)(2,1)} %copy.23.lowrank_w, bf16[16,1024]{1,0:T(8,128)(2,1)} %decay_w.1, f32[1,1024]{1,0:T(1,128)} %bitcast.1, ...), custom_call_target="tpu_custom_call" | custom-call | tf_op jit(solution)/shard_map/pallas_call | solution.py:346
  60.4 1.3 %copy.32 = bf16[16,512]{1,0:T(8,128)(2,1)} copy(bf16[16,512]{1,0:T(8,128)(2,1)} %get-tuple-element.4) | data formatting | bytes 32768
  61.8 4.6 %copy.33 = bf16[16,256,512]{2,1,0:T(8,128)(2,1)} copy(bf16[16,256,512]{2,1,0:T(8,128)(2,1)} %get-tuple-element.5) | data formatting | bytes 8388608
Async XLA Ops:
  9.0 4.0 %copy-start = (bf16[1,2048,480]{1,2,0:T(8,128)(2,1)S(1)}, bf16[1,2048,480]{1,2,0:T(8,128)(2,1)}, u32[]{:S(2)}) copy-start(bf16[1,2048,480]{1,2,0:T(8,128)(2,1)} %param.35) | copy-start | bytes 5898244
  15.5 4.0 %copy-start.1 = (bf16[2048,480]{0,1:T(8,128)(2,1)S(1)}, bf16[2048,480]{0,1:T(8,128)(2,1)}, u32[]{:S(2)}) copy-start(bf16[2048,480]{0,1:T(8,128)(2,1)} %param.38) | copy-start | bytes 5898244

commit v2 on v1

--- a/solution.py
+++ b/solution.py
@@ -19,19 +19,28 @@
 
 def norm_rows(floats, gain):
     scale = lax.rsqrt(jnp.mean(floats * floats, axis=-1, keepdims=True) + EPSILON)
-    return (floats * scale * gain.astype(F32)).astype(BF16)
+    return (floats * scale * gain).astype(BF16)
 
 
 def dot(left, right):
     return jnp.dot(left, right, preferred_element_type=F32)
+
+
+def dot_t(left, right):
+    return lax.dot_general(left, right, (((1,), (1,)), ((), ())), preferred_element_type=F32)
+
+
+def gain_row(gain_ref):
+    gain = gain_ref[...].astype(F32)
+    return jnp.concatenate([gain[i : i + 1, :] for i in range(gain.shape[0])], axis=1)
 
 
 def layer_kernel(
     n_ep, n_tp, heads,
     tokens, first_gain, lowrank_w, decay_w, decay_b, head_gain, second_gain, ids, weights,
     state_h, qw_h, kw_h, vw_h, gw_h, ow_h, eg_h, eu_h, ed_h, sg_h, su_h, sd_h,
-    out, new_state_h,
-    qw, kw, vw, gw, ow, eg, eu, ed, sg, su, sd, state, load_sem, store_sem,
+    out, state,
+    qw, kw, vw, gw, ow, eg, eu, ed, sg, su, sd, load_sem, share_t,
     normed, qk_part, qk_send, qk_recv, values, row_cols,
     at_send, at_recv, sq_send, sq_recv, second, rows_in, down_send, down_recv,
     sh_send, sh_recv, back_send, back_recv,
@@ -71,17 +80,18 @@
         (qw_h, qw), (kw_h, kw), (vw_h, vw), (gw_h, gw), (state_h, state), (ow_h, ow),
         (sg_h, sg), (su_h, su), (sd_h, sd), (eg_h.at[0], eg), (eu_h.at[0], eu), (ed_h.at[0], ed),
     ]
-    loads = {}
-    for i, (src, dst) in enumerate(sources):
-        copy = pltpu.make_async_copy(src, dst, load_sem.at[i])
-        copy.start()
-        loads[id(dst)] = copy
+    loads = {
+        id(dst): pltpu.make_async_copy(src, dst, load_sem.at[i])
+        for i, (src, dst) in enumerate(sources)
+    }
+    for src, dst in sources[:5]:
+        loads[id(dst)].start()
 
     def arrived(ref):
         loads[id(ref)].wait()
 
     tok = tokens[...].astype(F32)
-    nrm = norm_rows(tok, first_gain[...])
+    nrm = norm_rows(tok, gain_row(first_gain))
     normed[...] = nrm
     own = normed[:, pl.ds(pl.multiple_of(tp * feats, 128), feats)]
     qk_cols = heads * key_width
@@ -109,8 +119,11 @@
         cp.start()
         qk_copies.append(cp)
 
+    for src, dst in sources[5:]:
+        loads[id(dst)].start()
+
     offset = pl.multiple_of((tp * value_count // head_width) * key_width, 128)
-    lowrank = dot(nrm, lowrank_w[...]).astype(BF16)
+    lowrank = dot_t(nrm, lowrank_w[...]).astype(BF16)
     pre = dot(lowrank, decay_w[:, pl.ds(offset, key_width)]) + decay_b[:, pl.ds(offset, key_width)]
     log_decay = (jnp.minimum(pre, 0.0) - jnp.log1p(jnp.exp(-jnp.abs(pre)))) / 16.0
     decay = jnp.exp(log_decay)
@@ -119,7 +132,7 @@
     values[...] = val
     arrived(gw)
     gate = dot(nrm, gw[...]).astype(BF16).astype(F32)
-    gated = head_gain[...].astype(F32) * silu(gate)
+    gated = gain_row(head_gain) * silu(gate)
 
     q_own, k_own = qk_block(tp)
     query = q_own.astype(F32)
@@ -200,7 +213,7 @@
         attended = attended + at_recv[d].astype(F32)
     sec = (total + attended).astype(BF16)
     second[...] = sec
-    nrm2 = norm_rows(sec.astype(F32), second_gain[...])
+    nrm2 = norm_rows(sec.astype(F32), gain_row(second_gain))
     rows_in[0] = nrm2
 
     z_copies = []
@@ -217,7 +230,7 @@
 
     arrived(sg)
     arrived(su)
-    hid = (silu(dot(nrm2, sg[...])) * dot(nrm2, su[...])).astype(BF16)
+    hid = (silu(dot_t(nrm2, sg[...])) * dot_t(nrm2, su[...])).astype(BF16)
     arrived(sd)
     sh_copies = []
     for d in list(range(1, n_tp)) + [0]:
@@ -230,8 +243,6 @@
             sh_copies.append(cp)
 
     lax.fori_loop(half, batch, update, 0)
-    store = pltpu.make_async_copy(state, new_state_h, store_sem)
-    store.start()
 
     for dz in range(1, zs):
         z_copies[dz - 1].wait_recv()
@@ -247,7 +258,7 @@
         cp.wait_recv()
 
     x = rows_in[...].reshape(rows, width)
-    hidden = (silu(dot(x, eg[...])) * dot(x, eu[...])).astype(BF16)
+    hidden = (silu(dot_t(x, eg[...])) * dot_t(x, eu[...])).astype(BF16)
     down_copies = []
     for d in list(range(1, n_tp)) + [0]:
         peer = tp_peer(d)
@@ -277,8 +288,14 @@
         sh_copies[d - 1].wait_recv()
         shared = shared + sh_recv[d].astype(F32)
     result = shared + second[:, pl.ds(pl.multiple_of(tp * feats, 128), feats)].astype(F32)
-    id_vals = ids[...]
-    w_vals = weights[...]
+    number = lax.broadcasted_iota(jnp.int32, (128, batch), 0)
+    table = jnp.zeros((128, batch), F32)
+    for k in range(ids.shape[0]):
+        table = table + jnp.where(number == ids[k : k + 1, :], weights[k : k + 1, :], 0.0)
+    share_t[...] = jnp.zeros_like(share_t)
+    share_t[:, :batch] = table
+    shares = share_t[...].T[:batch]
+    expert_id = lax.broadcasted_iota(jnp.int32, (batch, 128), 1)
     for slot in range(n_ep):
         dz, r = slot // 2, slot % 2
         if slot == 0:
@@ -287,13 +304,12 @@
             back_copies[slot - 1].wait_recv()
             piece = back_recv[slot]
         expert = lax.rem(z + dz, zs) * 2 + (core if r == 0 else 1 - core)
-        share = jnp.sum(jnp.where(id_vals == expert, w_vals, 0.0), axis=1, keepdims=True)
+        share = jnp.sum(jnp.where(expert_id == expert, shares, 0.0), axis=1, keepdims=True)
         result = result + share * piece.astype(F32)
     out[...] = result.astype(BF16)
 
     for cp in qk_copies + at_copies + z_copies + c_copies + sh_copies + down_copies + back_copies:
         cp.wait_send()
-    store.wait()
 
 
 def body(
@@ -311,17 +327,16 @@
     rows = n_ep * batch
     zs = n_ep // 2
     vmem = pl.BlockSpec(memory_space=pltpu.VMEM)
-    hbm = pl.BlockSpec(memory_space=pl.ANY)
+    hbm = pl.BlockSpec(memory_space=pltpu.HBM)
     dma = pltpu.SemaphoreType.DMA
     big = [
         query_weight, key_weight, value_weight, outgate_weight, output_weight,
-        expert_gate[0], expert_up[0], expert_down[0], shared_gate, shared_up, shared_down,
+        expert_gate[0].T, expert_up[0].T, expert_down[0], shared_gate.T, shared_up.T, shared_down,
     ]
     scratch = [pltpu.VMEM(w.shape, BF16) for w in big]
     scratch += [
-        pltpu.VMEM(old_state.shape, BF16),
         dma((12,)),
-        dma,
+        pltpu.VMEM((128, 128), F32),
         pltpu.VMEM((batch, width), BF16),
         pltpu.VMEM((batch, 2 * qk_cols), BF16),
         pltpu.VMEM((n_tp, batch, 2 * key_width), BF16),
@@ -347,19 +362,20 @@
         functools.partial(layer_kernel, n_ep, n_tp, heads),
         out_shape=(
             jax.ShapeDtypeStruct((batch, feats), BF16),
-            jax.ShapeDtypeStruct(old_state.shape, BF16),
+            pltpu.VMEM(old_state.shape, BF16),
         ),
         in_specs=[vmem] * 9 + [hbm] * 12,
-        out_specs=(vmem, hbm),
+        out_specs=(vmem, vmem),
         scratch_shapes=scratch,
         compiler_params=pltpu.CompilerParams(
-            collective_id=0, has_side_effects=True, vmem_limit_bytes=60 * 1024 * 1024
+            collective_id=0, has_side_effects=True, vmem_limit_bytes=57 * 1024 * 1024
         ),
     )(
-        tokens, first_gain[None], lowrank_weight, decay_weight, decay_bias[None],
-        head_gain[None], second_gain[None], route_ids, route_weights,
+        tokens, first_gain.reshape(-1, 128), lowrank_weight.T, decay_weight, decay_bias[None],
+        head_gain.reshape(-1, 128), second_gain.reshape(-1, 128), route_ids.T, route_weights.T,
         old_state, query_weight, key_weight, value_weight, outgate_weight, output_weight,
-        expert_gate, expert_up, expert_down, shared_gate, shared_up, shared_down,
+        expert_gate.swapaxes(1, 2), expert_up.swapaxes(1, 2), expert_down,
+        shared_gate.T, shared_up.T, shared_down,
     )
     return layer_out, new_state
 

time: 66.8 us -> 42.3 us (0.63)
  local copies, waits for them, and re-layouts: 27.2 us -> 2.63 us
    unnamed x13 -> x4, local copies, waits for them, and re-layouts: 23.4 us -> 2.63 us
    broadcast_in_dim x3 -> x0, local copies, waits for them, and re-layouts: 3.83 us -> none  [the longest x1 1.29 us: body(): first_gain[None]]
where the time goes in v2:
time: 42.3 us; the launch traced here: 42.2 us
  Pallas kernels  38.9 us (92%)
  local copies, waits for them, and re-layouts  2.63 us (6%)
  between operations  0.66 us (2%)
    pallas_call x1, Pallas kernels, body(): pl.pallas_call(functools.partial(layer_kernel, n_ep, n_tp, heads), out_sh...  38.9 us
    unnamed x4, local copies, waits for them, and re-layouts  2.63 us

profile of v2, /device:TPU:0, one launch (start us, length us, event | category | flops | bytes accessed | tf_op | source)
XLA Modules:
  0.0 42.2 jit_solution(2666263253433258341)
XLA Ops:
  0.6 38.9 %shard_map.212 = (bf16[16,512]{1,0:T(8,128)(2,1)}, bf16[16,256,512]{2,1,0:T(8,128)(2,1)S(1)}) custom-call(bf16[16,2048]{1,0:T(8,128)(2,1)} %tokens.1, bf16[16,128]{1,0:T(8,128)(2,1)} %bitcast.16, bf16[16,2048]{1,0:T(8,128)(2,1)} %bitcast.15, bf16[16,1024]{1,0:T(8,128)(2,1)} %decay_w.1, f32[1,1024]{1,0:T(1,128)} %bitcast.17, bf16[4,128]{1,0:T(4,128)(2,1)} %bitcast.21, ...), custom_call_target="tpu_custom_call" | custom-call | tf_op jit(solution)/shard_map/pallas_call | solution.py:361
  39.5 0.0 copy-start
  39.6 2.0 %copy.25 = bf16[16,256,512]{2,1,0:T(8,128)(2,1)} copy(bf16[16,256,512]{2,1,0:T(8,128)(2,1)S(1)} %get-tuple-element.3) | data formatting | bytes 8388608
  41.6 0.0 copy-done
  41.6 0.6 %copy.26 = bf16[16,512]{1,0:T(8,128)(2,1)} copy(bf16[16,512]{1,0:T(8,128)(2,1)S(1)} %copy-done) | data formatting | bytes 32768
Async XLA Ops:
  39.5 2.0 %copy-start = (bf16[16,512]{1,0:T(8,128)(2,1)S(1)}, bf16[16,512]{1,0:T(8,128)(2,1)}, u32[]{:S(2)}) copy-start(bf16[16,512]{1,0:T(8,128)(2,1)} %get-tuple-element.6) | copy-start | bytes 49156

commit v3 on v2

--- a/solution.py
+++ b/solution.py
@@ -42,9 +42,9 @@
     out, state,
     qw, kw, vw, gw, ow, eg, eu, ed, sg, su, sd, load_sem, share_t,
     normed, qk_part, qk_send, qk_recv, values, row_cols,
-    at_send, at_recv, sq_send, sq_recv, second, rows_in, down_send, down_recv,
+    at_send, at_recv, sq_send, sq_recv, second, rows_in, kept, comb_send, comb_recv, down_send, down_recv,
     sh_send, sh_recv, back_send, back_recv,
-    qk_s, qk_r, at_s, at_r, sq_s, sq_r, z_s, z_r, c_s, c_r, dn_s, dn_r, sh_s, sh_r, bk_s, bk_r,
+    qk_s, qk_r, at_s, at_r, sq_s, sq_r, z_s, z_r, c_s, c_r, cb_s, cb_r, dn_s, dn_r, sh_s, sh_r, bk_s, bk_r,
 ):
     ep = lax.axis_index("ep")
     tp = lax.axis_index("tp")
@@ -54,13 +54,16 @@
     key_width, value_count = state.shape[1], state.shape[2]
     feats = width // n_tp
     head_width = value_count * n_tp // heads
-    rows = n_ep * batch
+    chunks = down_send.shape[0]
+    span = zs // chunks
 
     def tp_peer(d):
         return lax.rem(tp + d, n_tp)
 
-    def ep_at(dz, r):
-        return lax.rem(z - dz + zs, zs) * 2 + (core if r == 0 else 1 - core)
+    def along_z(dz):
+        return lax.rem(z + dz + zs, zs) * 2 + core
+
+    sibling = z * 2 + 1 - core
 
     def remote(src, dst, ssem, rsem, ep_to, tp_to):
         return pltpu.make_async_remote_copy(
@@ -71,10 +74,9 @@
     barrier = pltpu.get_barrier_semaphore()
     for d in range(1, n_tp):
         pl.semaphore_signal(barrier, inc=1, device_id=(ep, tp_peer(d)), device_id_type=MESH)
-    for d in range(1, n_ep):
-        pl.semaphore_signal(
-            barrier, inc=1, device_id=(lax.rem(ep + d, n_ep), tp), device_id_type=MESH
-        )
+    for dz in range(1, zs):
+        pl.semaphore_signal(barrier, inc=1, device_id=(along_z(dz), tp), device_id_type=MESH)
+    pl.semaphore_signal(barrier, inc=1, device_id=(sibling, tp), device_id_type=MESH)
 
     sources = [
         (qw_h, qw), (kw_h, kw), (vw_h, vw), (gw_h, gw), (state_h, state), (ow_h, ow),
@@ -107,7 +109,7 @@
             qk_part[:, pl.ds(pl.multiple_of(qk_cols + off, 128), key_width)],
         )
 
-    pl.semaphore_wait(barrier, n_tp - 1 + n_ep - 1)
+    pl.semaphore_wait(barrier, n_tp - 1 + zs)
 
     qk_copies = []
     for d in range(1, n_tp):
@@ -121,6 +123,16 @@
 
     for src, dst in sources[5:]:
         loads[id(dst)].start()
+
+    number = lax.broadcasted_iota(jnp.int32, (128, batch), 0)
+    table = jnp.zeros((128, batch), F32)
+    for k in range(ids.shape[0]):
+        table = table + jnp.where(number == ids[k : k + 1, :], weights[k : k + 1, :], 0.0)
+    part_high = table.astype(BF16).astype(F32)
+    share_t[...] = jnp.zeros_like(share_t)
+    share_t[:n_ep, :batch] = part_high[:n_ep]
+    share_t[n_ep : 2 * n_ep, :batch] = (table - part_high)[:n_ep]
+    rows_in[0, 0, :, width:] = share_t[...].T[:batch].astype(BF16)
 
     offset = pl.multiple_of((tp * value_count // head_width) * key_width, 128)
     lowrank = dot_t(nrm, lowrank_w[...]).astype(BF16)
@@ -214,19 +226,25 @@
     sec = (total + attended).astype(BF16)
     second[...] = sec
     nrm2 = norm_rows(sec.astype(F32), gain_row(second_gain))
-    rows_in[0] = nrm2
+    rows_in[0, 0, :, :width] = nrm2
 
     z_copies = []
     for dz in range(1, zs):
         cp = remote(
-            rows_in.at[0], rows_in.at[2 * dz], z_s.at[dz], z_r.at[dz],
-            lax.rem(z + dz, zs) * 2 + core, tp,
+            rows_in.at[0, 0], rows_in.at[0, dz], z_s.at[dz], z_r.at[dz], along_z(dz), tp
         )
         cp.start()
         z_copies.append(cp)
-    sibling = z * 2 + 1 - core
-    c_copies = [remote(rows_in.at[0], rows_in.at[1], c_s.at[0], c_r.at[0], sibling, tp)]
-    c_copies[0].start()
+    c_copies = []
+
+    def forward(dz):
+        if dz > 0:
+            z_copies[dz - 1].wait_recv()
+        cp = remote(rows_in.at[0, dz], rows_in.at[1, dz], c_s.at[dz], c_r.at[dz], sibling, tp)
+        cp.start()
+        c_copies.append(cp)
+
+    forward(0)
 
     arrived(sg)
     arrived(su)
@@ -244,71 +262,76 @@
 
     lax.fori_loop(half, batch, update, 0)
 
-    for dz in range(1, zs):
-        z_copies[dz - 1].wait_recv()
-        cp = remote(
-            rows_in.at[2 * dz], rows_in.at[2 * dz + 1], c_s.at[dz], c_r.at[dz], sibling, tp
-        )
+    comb_copies, down_copies = [], []
+
+    def expert_rows(r, lo):
+        x = rows_in[r, lo : lo + span]
+        x = x.reshape(span * batch, width + 128)
+        return x[:, :width], x[:, width:].astype(F32)
+
+    for ch in range(chunks):
+        lo = ch * span
+        for dz in range(max(lo, 1), lo + span):
+            forward(dz)
+        if ch == 0:
+            arrived(eg)
+            arrived(eu)
+            arrived(ed)
+        for dz in range(lo, lo + span):
+            c_copies[dz].wait_recv()
+        x1, w1 = expert_rows(1, lo)
+        x0, w0 = expert_rows(0, lo)
+        x = jnp.concatenate([x1, x0], axis=0)
+        w = jnp.concatenate([w1, w0], axis=0)
+        lane_id = lax.broadcasted_iota(jnp.int32, w.shape, 1)
+        mine = (lane_id == ep) | (lane_id == ep + n_ep)
+        share = jnp.sum(jnp.where(mine, w, 0.0), axis=1, keepdims=True)
+        hidden = (silu(dot_t(x, eg[...])) * dot_t(x, eu[...]) * share).astype(BF16)
+        comb_send[ch] = dot(hidden[: span * batch], ed[...]).astype(BF16)
+        cp = remote(comb_send.at[ch], comb_recv.at[ch], cb_s.at[ch], cb_r.at[ch], sibling, tp)
         cp.start()
-        c_copies.append(cp)
-    arrived(eg)
-    arrived(eu)
-    arrived(ed)
-    for cp in c_copies:
+        comb_copies.append(cp)
+        kept[...] = dot(hidden[span * batch :], ed[...])
         cp.wait_recv()
-
-    x = rows_in[...].reshape(rows, width)
-    hidden = (silu(dot_t(x, eg[...])) * dot_t(x, eu[...])).astype(BF16)
-    down_copies = []
-    for d in list(range(1, n_tp)) + [0]:
-        peer = tp_peer(d)
-        part = dot(hidden, ed[:, pl.ds(pl.multiple_of(peer * feats, 128), feats)]).astype(BF16)
-        down_send[d] = part
-        if d > 0:
-            cp = remote(down_send.at[d], down_recv.at[d], dn_s.at[d], dn_r.at[d], ep, peer)
+        for d in list(range(1, n_tp)) + [0]:
+            peer = tp_peer(d)
+            cols = pl.ds(pl.multiple_of(peer * feats, 128), feats)
+            down_send[ch, d] = (kept[:, cols] + comb_recv[ch, :, cols].astype(F32)).astype(BF16)
+            if d > 0:
+                cp = remote(
+                    down_send.at[ch, d], down_recv.at[ch, d],
+                    dn_s.at[ch, d], dn_r.at[ch, d], ep, peer,
+                )
+                cp.start()
+                down_copies.append(cp)
+
+    back_copies = []
+    for ch in range(chunks):
+        summed = down_send[ch, 0].astype(F32)
+        for d in range(1, n_tp):
+            down_copies[ch * (n_tp - 1) + d - 1].wait_recv()
+            summed = summed + down_recv[ch, d].astype(F32)
+        back_send[ch * span : (ch + 1) * span] = summed.astype(BF16).reshape(span, batch, feats)
+        for dz in range(max(ch * span, 1), (ch + 1) * span):
+            cp = remote(
+                back_send.at[dz], back_recv.at[dz], bk_s.at[dz], bk_r.at[dz], along_z(-dz), tp
+            )
             cp.start()
-            down_copies.append(cp)
-    summed = down_send[0].astype(F32)
-    for d in range(1, n_tp):
-        down_copies[d - 1].wait_recv()
-        summed = summed + down_recv[d].astype(F32)
-    back_send[...] = summed.astype(BF16).reshape(n_ep, batch, feats)
-
-    back_copies = []
-    for slot in range(1, n_ep):
-        dz, r = slot // 2, slot % 2
-        cp = remote(
-            back_send.at[slot], back_recv.at[slot], bk_s.at[slot], bk_r.at[slot], ep_at(dz, r), tp
-        )
-        cp.start()
-        back_copies.append(cp)
+            back_copies.append(cp)
 
     shared = sh_send[0].astype(F32)
     for d in range(1, n_tp):
         sh_copies[d - 1].wait_recv()
         shared = shared + sh_recv[d].astype(F32)
     result = shared + second[:, pl.ds(pl.multiple_of(tp * feats, 128), feats)].astype(F32)
-    number = lax.broadcasted_iota(jnp.int32, (128, batch), 0)
-    table = jnp.zeros((128, batch), F32)
-    for k in range(ids.shape[0]):
-        table = table + jnp.where(number == ids[k : k + 1, :], weights[k : k + 1, :], 0.0)
-    share_t[...] = jnp.zeros_like(share_t)
-    share_t[:, :batch] = table
-    shares = share_t[...].T[:batch]
-    expert_id = lax.broadcasted_iota(jnp.int32, (batch, 128), 1)
-    for slot in range(n_ep):
-        dz, r = slot // 2, slot % 2
-        if slot == 0:
-            piece = back_send[0]
-        else:
-            back_copies[slot - 1].wait_recv()
-            piece = back_recv[slot]
-        expert = lax.rem(z + dz, zs) * 2 + (core if r == 0 else 1 - core)
-        share = jnp.sum(jnp.where(expert_id == expert, shares, 0.0), axis=1, keepdims=True)
-        result = result + share * piece.astype(F32)
+    result = result + back_send[0].astype(F32)
+    for dz in range(1, zs):
+        back_copies[dz - 1].wait_recv()
+        result = result + back_recv[dz].astype(F32)
     out[...] = result.astype(BF16)
 
-    for cp in qk_copies + at_copies + z_copies + c_copies + sh_copies + down_copies + back_copies:
+    started = qk_copies + at_copies + z_copies + c_copies + sh_copies
+    for cp in started + comb_copies + down_copies + back_copies:
         cp.wait_send()
 
 
@@ -324,8 +347,9 @@
     heads = decay_weight.shape[1] // key_width
     feats = width // n_tp
     qk_cols = heads * key_width
-    rows = n_ep * batch
     zs = n_ep // 2
+    chunks = 2 if zs % 2 == 0 else 1
+    rows = zs * batch // chunks
     vmem = pl.BlockSpec(memory_space=pltpu.VMEM)
     hbm = pl.BlockSpec(memory_space=pltpu.HBM)
     dma = pltpu.SemaphoreType.DMA
@@ -348,16 +372,20 @@
         pltpu.VMEM((batch, 128), F32),
         pltpu.VMEM((n_tp, batch, 128), F32),
         pltpu.VMEM((batch, width), BF16),
-        pltpu.VMEM((n_ep, batch, width), BF16),
-        pltpu.VMEM((n_tp, rows, feats), BF16),
-        pltpu.VMEM((n_tp, rows, feats), BF16),
+        pltpu.VMEM((2, zs, batch, width + 128), BF16),
+        pltpu.VMEM((rows, width), F32),
+        pltpu.VMEM((chunks, rows, width), BF16),
+        pltpu.VMEM((chunks, rows, width), BF16),
+        pltpu.VMEM((chunks, n_tp, rows, feats), BF16),
+        pltpu.VMEM((chunks, n_tp, rows, feats), BF16),
         pltpu.VMEM((n_tp, batch, feats), BF16),
         pltpu.VMEM((n_tp, batch, feats), BF16),
-        pltpu.VMEM((n_ep, batch, feats), BF16),
-        pltpu.VMEM((n_ep, batch, feats), BF16),
+        pltpu.VMEM((zs, batch, feats), BF16),
+        pltpu.VMEM((zs, batch, feats), BF16),
     ]
-    for count in (n_tp, n_tp, n_tp, zs, zs, n_tp, n_tp, n_ep):
-        scratch += [dma((count,)), dma((count,))]
+    counts = ((n_tp,), (n_tp,), (n_tp,), (zs,), (zs,), (chunks,), (chunks, n_tp), (n_tp,), (zs,))
+    for count in counts:
+        scratch += [dma(count), dma(count)]
     layer_out, new_state = pl.pallas_call(
         functools.partial(layer_kernel, n_ep, n_tp, heads),
         out_shape=(

time: 42.3 us -> 39.6 us (0.936)
  Pallas kernels: 38.9 us -> 36.1 us
    pallas_call x1, Pallas kernels: 38.9 us -> 36.1 us  [body(): pl.pallas_call(functools.partial(layer_kernel, n_ep, n_tp, heads), out_sh...]
where the time goes in v3:
time: 39.6 us; the launch traced here: 39.4 us
  Pallas kernels  36.1 us (91%)
  local copies, waits for them, and re-layouts  2.63 us (7%)
  between operations  0.66 us (2%)
    pallas_call x1, Pallas kernels, body(): pl.pallas_call(functools.partial(layer_kernel, n_ep, n_tp, heads), out_sh...  36.1 us
    unnamed x4, local copies, waits for them, and re-layouts  2.63 us

profile of v3, /device:TPU:0, one launch (start us, length us, event | category | flops | bytes accessed | tf_op | source)
XLA Modules:
  0.0 39.4 jit_solution(6101881991195417220)
XLA Ops:
  0.6 36.1 %shard_map.212 = (bf16[16,512]{1,0:T(8,128)(2,1)}, bf16[16,256,512]{2,1,0:T(8,128)(2,1)S(1)}) custom-call(bf16[16,2048]{1,0:T(8,128)(2,1)} %tokens.1, bf16[16,128]{1,0:T(8,128)(2,1)} %bitcast.16, bf16[16,2048]{1,0:T(8,128)(2,1)} %bitcast.15, bf16[16,1024]{1,0:T(8,128)(2,1)} %decay_w.1, f32[1,1024]{1,0:T(1,128)} %bitcast.17, bf16[4,128]{1,0:T(4,128)(2,1)} %bitcast.21, ...), custom_call_target="tpu_custom_call" | custom-call | tf_op jit(solution)/shard_map/pallas_call | solution.py:389
  36.8 0.0 copy-start
  36.8 2.0 %copy.25 = bf16[16,256,512]{2,1,0:T(8,128)(2,1)} copy(bf16[16,256,512]{2,1,0:T(8,128)(2,1)S(1)} %get-tuple-element.3) | data formatting | bytes 8388608
  38.8 0.0 copy-done
  38.8 0.6 %copy.26 = bf16[16,512]{1,0:T(8,128)(2,1)} copy(bf16[16,512]{1,0:T(8,128)(2,1)S(1)} %copy-done) | data formatting | bytes 32768
Async XLA Ops:
  36.8 2.0 %copy-start = (bf16[16,512]{1,0:T(8,128)(2,1)S(1)}, bf16[16,512]{1,0:T(8,128)(2,1)}, u32[]{:S(2)}) copy-start(bf16[16,512]{1,0:T(8,128)(2,1)} %get-tuple-element.6) | copy-start | bytes 49156
